TPU v7x, 512 devices: a whole 4x8x8 slice. The times are simulated.
512 devices in a mesh: sp: 32 (over z, x), tp: 16 (over y, core).
Axes of the slice: x: 4, y: 8, z: 8, core: 2. Of those that a mesh axis runs over, the one named last changes fastest.
Arguments:
- latent: bfloat16 [16384, 2048], P('sp'), may hold values from -6 to 6
- context: bfloat16 [512, 2048], P('sp'), may hold values from -6 to 6
- condition: bfloat16 [2048], replicated, may hold values from -6 to 6
- context_condition: bfloat16 [2048], replicated, may hold values from -6 to 6
- shift_weight: bfloat16 [2048, 2048], P('sp', 'tp'), may hold values from -0.125 to 0.125
- scale_weight: bfloat16 [2048, 2048], P('sp', 'tp'), may hold values from -0.125 to 0.125
- mod_gate_weight: bfloat16 [2048, 2048], P('sp', 'tp'), may hold values from -0.5 to 0.5
- norm_gain: bfloat16 [2048], replicated, may hold values from 0.099609375 to 1.8984375
- query_weight: bfloat16 [2048, 2048], P(None, 'tp'), may hold values from -0.125 to 0.125
- key_weight: bfloat16 [2048, 2048], P(None, 'tp'), may hold values from -0.125 to 0.125
- value_weight: bfloat16 [2048, 2048], P(None, 'tp'), may hold values from -0.125 to 0.125
- gate_weight: bfloat16 [2048, 2048], P(None, 'tp'), may hold values from -0.125 to 0.125
- forward_decay: float32 [16], P('tp'), may hold values from 0 to 1, as said below
- backward_decay: float32 [16], P('tp'), may hold values from 0 to 1, as said below
- out_weight: bfloat16 [2048, 2048], P('tp'), may hold values from -0.125 to 0.125
Outputs:
- mixed: bfloat16 [16384, 2048], P('sp')
Inputs may be any that keep to these rules, and one draw needn't show every extreme that they name: `forward_decay`: each head's rate is positive. `backward_decay`: each head's rate is positive.
All inputs are finite; a program needn't handle non-finite values.
Results may differ from a plain program's by a relative error of at most 0.015.
Values may be sent and summed in bfloat16 or wider, within the bound.
No kernel may reach another device: no remote copies, remote signals or barrier semaphores. Data moves between devices by JAX's collectives and lax.ppermute only.
A program may use at most 64 MiB of HBM per device.

v0:
```python
import jax
import jax.numpy as jnp
from jax import lax
from jax.sharding import Mesh
from jax.sharding import PartitionSpec as P

HEAD_DIM = 128
GRID_W = 64
SP = ("sp_0", "sp_1")


EPS = 1e-06
THETA = 10000.0
CONTEXT_LIFT = 3.0
TOP_PRECISION = lax.Precision.HIGHEST


def sent_to_all(x, axis):
    copies = jnp.broadcast_to(x, (lax.axis_size(axis), *x.shape))
    return lax.all_to_all(copies, axis, split_axis=0, concat_axis=0, tiled=True)


def taken_together(x, axis):
    everything = sent_to_all(x, axis)
    return jnp.sum(everything, axis=0)


def in_one(arrays, axis):
    ravelled, at, finished = (jnp.concatenate([a.reshape(-1) for a in arrays]), 0, [])
    total = lax.psum(ravelled, axis)
    for a in arrays:
        finished.append(total[at : at + a.size].reshape(a.shape))
        at += a.size
    return tuple(finished)


def filled_with(x, identity):
    return jax.tree.map(
        lambda a, e: jnp.broadcast_to(jnp.asarray(e, a.dtype), a.shape), x, identity
    )


def all_in_one(x, axis):
    leaves = jax.tree.leaves(x)
    order = sorted(range(len(leaves)), key=lambda k: -leaves[k].size)
    width = (1, *leaves[order[0]].shape)[-1]
    lines = [
        jnp.pad(leaves[k].reshape(-1), (0, -leaves[k].size % width)).reshape(-1, width)
        for k in order
    ]
    both, at, found = (lax.all_gather(jnp.concatenate(lines), axis), 0, {})
    for k, line in zip(order, lines):
        slab = both[:, at : at + len(line)].reshape(len(both), -1)
        found[k] = slab[:, : leaves[k].size].reshape(-1, *leaves[k].shape)
        at += len(line)
    numbers = iter(range(len(leaves)))
    return jax.tree.map(lambda _: found[next(numbers)], x)


def prefix_by_axis(x, axes, combine, identity, reverse):
    before = start = filled_with(x, identity)
    total = x
    for axis in reversed(axes):
        length, mine = (lax.axis_size(axis), lax.axis_index(axis))
        pieces = all_in_one(total, axis)
        inside, total = (start, start)
        for k in reversed(range(length)) if reverse else range(length):
            passed = k > mine if reverse else k < mine
            total = combine(total, jax.tree.map(lambda part: part[k], pieces))
            inside = jax.tree.map(lambda new, old: jnp.where(passed, new, old), total, inside)
        before = combine(inside, before)
    return before


def laid_out(parts, dim):
    dims = list(parts.shape[1:])
    dims[dim] *= parts.shape[0]
    return jnp.moveaxis(parts, 0, dim).reshape(dims)


def collect(x, axis, dim):
    return laid_out(sent_to_all(x, axis), dim)


def modulated(token_rows, norm_gain, shifts, scales):
    values = token_rows.astype(jnp.float32)
    values = values * lax.rsqrt(jnp.mean(values * values, axis=-1, keepdims=True) + EPS)
    values = values * norm_gain.astype(jnp.float32)
    return (values * (1.0 + scales) + shifts).astype(jnp.bfloat16)


def rope_half(portion, positions):
    quarter = portion.shape[-1] // 2
    frequency = THETA ** (-jnp.arange(quarter, dtype=jnp.float32) / quarter)
    angles = positions[:, None, None] * frequency
    cosine = jnp.cos(angles)
    sine_table = jnp.sin(angles)
    leading = portion[..., :quarter]
    trailing = portion[..., quarter:]
    return jnp.concatenate(
        [leading * cosine - trailing * sine_table, leading * sine_table + trailing * cosine],
        axis=-1,
    )


def rotate(values, grid_row, grid_column):
    half_width = values.shape[-1] // 2
    return jnp.concatenate(
        [
            rope_half(values[..., :half_width], grid_row),
            rope_half(values[..., half_width:], grid_column),
        ],
        axis=-1,
    )


def combine(earlier, later):
    return (earlier[0] * later[0], later[0][:, None, None] * earlier[1] + later[1])


def local(
    latent,
    context,
    condition,
    context_condition,
    shift_weight,
    scale_weight,
    mod_gate_weight,
    norm_gain,
    query_weight,
    key_weight,
    value_weight,
    gate_weight,
    forward_decay,
    backward_decay,
    out_weight,
):
    sp_index = lax.axis_index(SP)
    tp_index = lax.axis_index("tp")
    sp_count = lax.axis_size(SP)
    tp_count = lax.axis_size("tp")
    tokens_here = latent.shape[0]
    local_rows = tokens_here // tp_count
    mod_rows = shift_weight.shape[0]
    activation = jax.nn.silu(jnp.stack([condition, context_condition]).astype(jnp.float32)).astype(
        jnp.bfloat16
    )
    own_part = lax.dynamic_slice_in_dim(activation, sp_index * mod_rows, mod_rows, 1)
    partial_value = jnp.stack(
        [
            jnp.dot(own_part, matrix, preferred_element_type=jnp.float32)
            for matrix in (shift_weight, scale_weight, mod_gate_weight)
        ]
    )
    summed = taken_together(partial_value, SP)
    modulation = lax.all_gather(summed, "tp", axis=2, tiled=True)
    hidden = modulated(latent, norm_gain, modulation[0, 0], modulation[1, 0])
    context_hidden = modulated(context, norm_gain, modulation[0, 1], modulation[1, 1])
    local_width = query_weight.shape[1]
    head_count = local_width // HEAD_DIM
    stacked = jnp.concatenate([query_weight, key_weight, value_weight, gate_weight], axis=1)
    projected = jnp.dot(hidden, stacked, preferred_element_type=jnp.float32).astype(jnp.bfloat16)
    queries = projected[:, :local_width]
    keys_out = projected[:, local_width : 2 * local_width]
    values_out = projected[:, 2 * local_width : 3 * local_width]
    out_gates = projected[:, 3 * local_width :]
    context_pairs = jnp.dot(
        context_hidden,
        stacked[:, local_width : 3 * local_width],
        preferred_element_type=jnp.float32,
    ).astype(jnp.bfloat16)

    def to_heads(values):
        return values.astype(jnp.float32).reshape(values.shape[0], head_count, HEAD_DIM)

    positions = sp_index * tokens_here + jnp.arange(tokens_here, dtype=jnp.int32)
    grid_row = (positions // GRID_W).astype(jnp.float32)
    grid_column = (positions % GRID_W).astype(jnp.float32)
    key_scale = HEAD_DIM ** (-0.5)
    query_heads = jnp.transpose(rotate(to_heads(queries), grid_row, grid_column), (1, 0, 2))
    key_heads = (
        jnp.transpose(rotate(to_heads(keys_out), grid_row, grid_column), (1, 0, 2)) * key_scale
    )
    value_heads = jnp.transpose(to_heads(values_out), (1, 0, 2))
    log_forward = -forward_decay
    log_backward = -backward_decay
    context_rows = context.shape[0]
    context_total = context_rows * sp_count
    context_index = (sp_index * context_rows + jnp.arange(context_rows, dtype=jnp.int32)).astype(
        jnp.float32
    )
    weight_forward = jnp.exp(log_forward[:, None] * (context_total - 1.0 - context_index)[None, :])
    weight_backward = jnp.exp(log_backward[:, None] * context_index[None, :])
    context_key_heads = to_heads(context_pairs[:, :local_width]) * (key_scale * CONTEXT_LIFT)
    context_value_heads = to_heads(context_pairs[:, local_width:])
    context_forward = jnp.einsum(
        "hc,chd,che->hde",
        weight_forward,
        context_key_heads,
        context_value_heads,
        precision=TOP_PRECISION,
    )
    context_backward = jnp.einsum(
        "hc,chd,che->hde",
        weight_backward,
        context_key_heads,
        context_value_heads,
        precision=TOP_PRECISION,
    )
    context_forward, context_backward = in_one((context_forward, context_backward), SP)
    offsets = jnp.arange(tokens_here, dtype=jnp.float32)
    distance = offsets[:, None] - offsets[None, :]
    mixing = jnp.where(
        distance >= 0, jnp.exp(log_forward[:, None, None] * jnp.maximum(distance, 0.0)), 0.0
    )
    mixing = mixing + jnp.where(
        distance <= 0, jnp.exp(log_backward[:, None, None] * jnp.maximum(-distance, 0.0)), 0.0
    )
    score_matrix = (
        jnp.einsum("htd,hsd->hts", query_heads, key_heads, precision=TOP_PRECISION) * mixing
    )
    local_out = jnp.einsum("hts,hse->hte", score_matrix, value_heads, precision=TOP_PRECISION)
    tail_forward = jnp.exp(log_forward[:, None] * (tokens_here - 1.0 - offsets)[None, :])
    head_backward = jnp.exp(log_backward[:, None] * offsets[None, :])
    own_forward = jnp.einsum(
        "ht,htd,hte->hde", tail_forward, key_heads, value_heads, precision=TOP_PRECISION
    )
    own_backward = jnp.einsum(
        "ht,htd,hte->hde", head_backward, key_heads, value_heads, precision=TOP_PRECISION
    )
    span_forward = jnp.exp(log_forward * tokens_here)
    span_backward = jnp.exp(log_backward * tokens_here)
    identity = (jnp.ones_like(span_forward), jnp.zeros_like(own_forward))
    before = prefix_by_axis((span_forward, own_forward), SP, combine, identity, False)
    after = prefix_by_axis((span_backward, own_backward), SP, combine, identity, True)
    device_start = (sp_index * tokens_here).astype(jnp.float32)
    device_rest = ((sp_count - 1 - sp_index) * tokens_here).astype(jnp.float32)
    incoming_forward = (
        before[1] + jnp.exp(log_forward * device_start)[:, None, None] * context_forward
    )
    incoming_backward = (
        after[1] + jnp.exp(log_backward * device_rest)[:, None, None] * context_backward
    )
    read_forward = jnp.exp(log_forward[:, None] * (offsets + 1.0)[None, :])[
        :, :, None
    ] * jnp.einsum("htd,hde->hte", query_heads, incoming_forward, precision=TOP_PRECISION)
    read_backward = jnp.exp(log_backward[:, None] * (tokens_here - offsets)[None, :])[
        :, :, None
    ] * jnp.einsum("htd,hde->hte", query_heads, incoming_backward, precision=TOP_PRECISION)
    retained = local_out + read_forward + read_backward
    retained = retained * lax.rsqrt(jnp.mean(retained * retained, axis=-1, keepdims=True) + EPS)
    merged = jnp.transpose(retained, (1, 0, 2)).reshape(tokens_here, local_width)
    heads_out = (jax.nn.silu(out_gates.astype(jnp.float32)) * merged).astype(jnp.bfloat16)
    projection = lax.psum_scatter(
        jnp.dot(heads_out, out_weight, preferred_element_type=jnp.float32),
        "tp",
        scatter_dimension=0,
        tiled=True,
    )
    own_latent = lax.dynamic_slice_in_dim(latent, tp_index * local_rows, local_rows, 0)
    finished = (own_latent.astype(jnp.float32) + modulation[2, 0] * projection).astype(jnp.bfloat16)
    return collect(finished, "tp", 0)


def solution(mesh):
    torus = Mesh(mesh.devices.reshape(8, 4, mesh.shape["tp"]), ("sp_0", "sp_1", "tp"))
    in_specs = (
        P(SP, None),
        P(SP, None),
        P(),
        P(),
        P(SP, "tp"),
        P(SP, "tp"),
        P(SP, "tp"),
        P(),
        P(None, "tp"),
        P(None, "tp"),
        P(None, "tp"),
        P(None, "tp"),
        P("tp"),
        P("tp"),
        P("tp", None),
    )
    out_specs = P(SP, None)
    return jax.shard_map(local, mesh=torus, in_specs=in_specs, out_specs=out_specs, check_vma=False)
```

profile of v0, /device:TPU:1, one launch (start us, length us, event | category | flops | bytes accessed | tf_op | source)
XLA Modules:
  0.0 352.9 jit_solution(17837896909596042663)
XLA Ops:
  6.5 0.0 copy-start
  6.5 0.8 stack.21
  7.4 0.7 stack.22
  8.1 0.9 convolution_bitcast_fusion.4
  9.0 0.9 convolution_bitcast_fusion.3
  9.9 0.9 convolution_bitcast_fusion.2
  10.9 0.7 broadcast_in_dim.10
  11.5 13.7 %all-to-all-start = ((f32[32,3,2,128]{3,2,1,0:T(2,128)}), f32[32,3,2,128]{3,2,1,0:T(2,128)S(1)}, u32[]{:S(2)}, u32[]{:S(2)}) async-start(f32[32,3,2,128]{3,2,1,0:T(2,128)} %broadcast_in_dim.10), calls=%async_computation | async-start | bytes 196608 | tf_op jit(solution)/shard_map/all_to_all | solution.py:20
  25.3 0.0 all-reduce.6.cloned.1.call-start
  27.0 1.0 fusion.45
  28.0 2.1 fusion
  30.0 0.7 convert_element_type.83
  30.7 3.6 %all-to-all-done = f32[32,3,2,128]{3,2,1,0:T(2,128)S(1)} async-done(((f32[32,3,2,128]{3,2,1,0:T(2,128)}), f32[32,3,2,128]{3,2,1,0:T(2,128)S(1)}, u32[]{:S(2)}, u32[]{:S(2)}) %all-to-all-start) | async-done | bytes 98336 | tf_op jit(solution)/shard_map/all_to_all | solution.py:20
  34.4 0.1 reduce_sum.36
  34.4 19.6 %all_gather.27 = f32[3,2,2048]{2,1,0:T(2,128)S(1)} all-gather(f32[3,2,128]{2,1,0:T(2,128)S(1)} %reduce_sum.36), channel_id=1, replica_groups=mesh['sp_0'=8,'sp_1'=4,'tp'=16] {'tp'}, dimensions={2}, use_global_device_ids=true | all-gather | bytes 52224 | tf_op jit(solution)/shard_map/all_gather | solution.py:156
  54.1 1.5 convolution_convert_fusion
  55.6 0.3 convolution_bitcast_fusion.1
  55.9 0.3 convolution_bitcast_fusion
  56.2 0.7 pad_maximum_fusion
  56.9 0.0 all-reduce.6.cloned.1.call-update
  56.9 0.0 reduce-scatter.2.cloned.1.call-start
  57.0 2.9 fusion.18
  59.9 0.1 fusion.53
  60.0 0.6 fusion.82
  60.6 0.3 fusion.40
  60.8 0.3 fusion.42
  61.1 9.4 %all-gather.4 = f32[4,129,128]{2,1,0:T(8,128)S(1)} all-gather(f32[1,129,128]{2,1,0:T(8,128)S(1)} %maximum_bitcast_fusion.4), channel_id=2, replica_groups=mesh['sp_0'=8,'sp_1'=4,'tp'=16] {'sp_1'}, dimensions={0}, use_global_device_ids=true | all-gather | bytes 330240 | tf_op jit(solution)/shard_map/all_gather | solution.py:51
  70.6 0.6 fusion.227
  74.4 9.7 %all-gather.6 = f32[4,129,128]{2,1,0:T(8,128)S(1)} all-gather(f32[1,129,128]{2,1,0:T(8,128)S(1)} %maximum_bitcast_fusion.6), channel_id=4, replica_groups=mesh['sp_0'=8,'sp_1'=4,'tp'=16] {'sp_1'}, dimensions={0}, use_global_device_ids=true | all-gather | bytes 330240 | tf_op jit(solution)/shard_map/all_gather | solution.py:51
  84.1 0.6 fusion.226
  89.2 2.0 fusion.233
  91.1 19.6 %all-gather.7 = f32[8,129,128]{2,1,0:T(8,128)S(1)} all-gather(f32[1,129,128]{2,1,0:T(8,128)S(1)} %maximum_bitcast_fusion.7), channel_id=5, replica_groups=mesh['sp_0'=8,'sp_1'=4,'tp'=16] {'sp_0'}, dimensions={0}, use_global_device_ids=true | all-gather | bytes 594432 | tf_op jit(solution)/shard_map/all_gather | solution.py:51
  110.7 0.7 fusion.224
  111.4 1.9 fusion.234
  113.3 20.3 %all-gather.5 = f32[8,129,128]{2,1,0:T(8,128)S(1)} all-gather(f32[1,129,128]{2,1,0:T(8,128)S(1)} %maximum_bitcast_fusion.5), channel_id=3, replica_groups=mesh['sp_0'=8,'sp_1'=4,'tp'=16] {'sp_0'}, dimensions={0}, use_global_device_ids=true | all-gather | bytes 594432 | tf_op jit(solution)/shard_map/all_gather | solution.py:51
  133.7 0.7 fusion.225
  135.6 1.5 convolution_multiply_fusion
  137.2 0.7 fusion.62
  137.9 61.9 %all-reduce.6.cloned.1.call-done = f32[32768]{0:T(1024)} async-done(((f32[32768]{0:T(1024)}), f32[32768]{0:T(1024)}) %all-reduce.6.cloned.1.call-update) | async-done | bytes 131088 | tf_op jit(solution)/shard_map/psum | solution.py:30
  199.9 8.0 %fusion.24 = f32[512,128]{0,1:T(8,128)S(1)} fusion(f32[512,128]{0,1:T(8,128)S(1)} %fusion.62, f32[512]{0:T(512)S(1)} %multiply_exponential_fusion.1, f32[32768]{0:T(1024)} %all-reduce.6.cloned.1.call-done, f32[8,129,128]{2,1,0:T(8,128)} %copy-done.3, f32[4,129,128]{2,1,0:T(8,128)S(1)} %all-gather.4, f32[512,1,32]{0,2,1:T(8,128)} %copy-done.5, ...), kind=kOutput, calls=%fused_computation.26 | convolution fusion | flops 101695488 | bytes 1847816 | tf_op jit(solution)/shard_map/htd,hde->hte/dot_general | solution.py:246
  207.9 8.0 %multiply_reduce_fusion = (f32[512]{0:T(512)S(1)}, f32[512,128]{0,1:T(8,128)S(1)}) fusion(f32[512,128]{0,1:T(8,128)S(1)} %fusion.24, f32[32768]{0:T(1024)} %all-reduce.6.cloned.1.call-done, f32[8,129,128]{2,1,0:T(8,128)} %copy-done.2, f32[4,129,128]{2,1,0:T(8,128)S(1)} %all-gather.6, f32[]{:T(128)} %bitcast.75, f32[]{:T(128)} %bitcast.76, f32[]{:T(128)} %bitcast.77, ...), kind=kOutput, calls=%fused_computation.53 | convolution fusion | flops 101826048 | bytes 1849864 | tf_op jit(solution)/shard_map/htd,hde->hte/dot_general | solution.py:249
  215.9 3.6 %fusion.50 = f32[512,2048]{1,0:T(8,128)} fusion(bf16[128,2048]{1,0:T(8,128)(2,1)S(1)} %copy-done, f32[512,128]{0,1:T(8,128)S(1)} %get-tuple-element.53, bf16[512,512]{0,1:T(8,128)(2,1)} %copy-done.4, f32[512]{0:T(512)S(1)} %add_rsqrt_fusion), kind=kOutput, calls=%fused_computation.66 | convolution fusion | flops 268959744 | bytes 5113856 | tf_op jit(solution)/shard_map/dot_general | solution.py:255
  219.5 0.0 reduce-scatter.2.cloned.1.call-update
  219.5 66.3 %reduce-scatter.2.cloned.1.call-done = f32[32,2048]{1,0:T(8,128)} async-done(((f32[512,2048]{1,0:T(8,128)}), f32[32,2048]{1,0:T(8,128)}) %reduce-scatter.2.cloned.1.call-update) | async-done | bytes 262160 | tf_op jit(solution)/shard_map/reduce_scatter | solution.py:254
  285.8 1.0 add_convert_fusion
  286.8 0.2 broadcast_in_dim.12
  287.1 57.7 %all_to_all.10 = bf16[16,32,2048]{2,1,0:T(8,128)(2,1)S(1)} all-to-all(bf16[16,32,2048]{2,1,0:T(8,128)(2,1)S(1)} %broadcast_in_dim.12), channel_id=1, replica_groups=mesh['sp_0'=8,'sp_1'=4,'tp'=16] {'tp'}, dimensions={0} | all-to-all | bytes 4194304 | tf_op jit(solution)/shard_map/all_to_all | solution.py:20
  344.8 1.3 copy.34
  (42 shorter events, 0.3 us)
Async XLA Ops:
  6.5 209.4 %copy-start = (bf16[128,2048]{1,0:T(8,128)(2,1)S(1)}, bf16[128,2048]{1,0:T(8,128)(2,1)}, u32[]{:S(2)}) copy-start(bf16[128,2048]{1,0:T(8,128)(2,1)} %param.29) | copy-start | bytes 1572868
  6.5 50.4 %copy-start.1 = (bf16[512,2048]{1,0:T(8,128)(2,1)S(1)}, bf16[512,2048]{1,0:T(8,128)(2,1)}, u32[]{:S(2)}) copy-start(bf16[512,2048]{1,0:T(8,128)(2,1)} %param.15) | copy-start | bytes 6291460
  6.5 50.4 %copy-start.8 = (bf16[2048,128]{1,0:T(8,128)(2,1)S(1)}, bf16[2048,128]{1,0:T(8,128)(2,1)}, u32[]{:S(2)}) copy-start(bf16[2048,128]{1,0:T(8,128)(2,1)} %param.25) | copy-start | bytes 1572868
  11.5 22.8 %all-to-all-start = ((f32[32,3,2,128]{3,2,1,0:T(2,128)}), f32[32,3,2,128]{3,2,1,0:T(2,128)S(1)}, u32[]{:S(2)}, u32[]{:S(2)}) async-start(f32[32,3,2,128]{3,2,1,0:T(2,128)} %broadcast_in_dim.10), calls=%async_computation | async-start | bytes 196608 | tf_op jit(solution)/shard_map/all_to_all | solution.py:20
  25.3 174.6 %all-reduce.6.cloned.1.call-start = ((), (), s32[]{:S(2)}) async-start(), calls=%async_computation.3 | async-start | bytes 262144 | tf_op jit(solution)/shard_map/psum | solution.py:30
  56.9 228.9 %reduce-scatter.2.cloned.1.call-start = ((), (), s32[]{:S(2)}) async-start(), calls=%async_computation.4 | async-start | bytes 4456448 | tf_op jit(solution)/shard_map/reduce_scatter | solution.py:254
  59.9 77.3 %copy-start.4 = (bf16[512,512]{0,1:T(8,128)(2,1)}, bf16[512,512]{0,1:T(8,128)(2,1)S(1)}, u32[]{:S(2)}) copy-start(bf16[512,512]{0,1:T(8,128)(2,1)S(1)} %fusion.18) | copy-start | bytes 1572868
  60.5 76.6 %copy-start.5 = (f32[512,1,32]{0,2,1:T(8,128)}, f32[512,1,32]{0,2,1:T(8,128)S(1)}, u32[]{:S(2)}) copy-start(f32[512,1,32]{0,2,1:T(8,128)S(1)} %get-tuple-element.25) | copy-start | bytes 196612
  60.5 76.6 %copy-start.6 = (f32[512,1,32]{0,2,1:T(8,128)}, f32[512,1,32]{0,2,1:T(8,128)S(1)}, u32[]{:S(2)}) copy-start(f32[512,1,32]{0,2,1:T(8,128)S(1)} %get-tuple-element.26) | copy-start | bytes 196612
  60.6 76.6 %copy-start.7 = (f32[512,1,32]{0,2,1:T(8,128)}, f32[512,1,32]{0,2,1:T(8,128)S(1)}, u32[]{:S(2)}) copy-start(f32[512,1,32]{0,2,1:T(8,128)S(1)} %get-tuple-element.27) | copy-start | bytes 196612
  110.7 24.9 %copy-start.2 = (f32[8,129,128]{2,1,0:T(8,128)}, f32[8,129,128]{2,1,0:T(8,128)S(1)}, u32[]{:S(2)}) copy-start(f32[8,129,128]{2,1,0:T(8,128)S(1)} %all-gather.7) | copy-start | bytes 1585156
  133.7 2.0 copy-start.3
Sparse Core Ops, SparseCore 0:
  57.0 142.7 all-reduce.5
  219.6 66.1 reduce-scatter.1
where the time goes:
time: 354 us; the launch traced here: 353 us
  blocking collectives  136 us (38%)
  waiting for transfers between devices  132 us (37%)
  matrix products  30.2 us (9%)
  between operations  24.2 us (7%)
  starting transfers between devices  13.8 us (4%)
  other arithmetic  10.1 us (3%)
  local copies, waits for them, and re-layouts  6.43 us (2%)
    reduce_scatter x1, waiting for transfers between devices, local(): lax.psum_scatter(jnp.dot(heads_out, out_weight, preferred_element_type=jn...  66.3 us
    psum x1, waiting for transfers between devices, in_one(): total = lax.psum(ravelled, axis)  61.9 us
    all_gather x4, blocking collectives, all_in_one(): both, at, found = (lax.all_gather(jnp.concatenate(lines), axis), 0, {})  59 us
    all_to_all x1, blocking collectives, sent_to_all(): return lax.all_to_all(copies, axis, split_axis=0, concat_axis=0, tiled=True)  57.7 us
    all_gather x1, blocking collectives, local(): modulation = lax.all_gather(summed, 'tp', axis=2, tiled=True)  19.6 us
    all_to_all x1, starting transfers between devices, sent_to_all(): return lax.all_to_all(copies, axis, split_axis=0, concat_axis=0, tiled=True)  13.7 us
    dot_general x1, matrix products, local(): jnp.einsum('htd,hde->hte', query_heads, incoming_forward, precision=TOP_P...  8.03 us
    dot_general x1, matrix products, local(): jnp.einsum('htd,hde->hte', query_heads, incoming_backward, precision=TOP_...  7.98 us
  transfers between devices with their start and end apart: 3, of which 3 were waited for; matrix products, arithmetic and copies ran while one was open for 5% of the time, Pallas kernels for 0%

commit v1 on v0

v1 whole, which is shorter than its diff:
```python
import jax
import jax.numpy as jnp
from jax import lax
from jax.experimental import pallas as pl
from jax.experimental.pallas import tpu as pltpu
from jax.sharding import Mesh
from jax.sharding import PartitionSpec as P

HEAD_DIM = 128
GRID_W = 64
SP = ("z", "x")
TP = ("y", "c")
EPS = 1e-06
THETA = 10000.0
CONTEXT_LIFT = 3.0
BF = jnp.bfloat16
F32 = jnp.float32


def dot(a, b, dims):
    return lax.dot_general(a, b, (dims, ((), ())), preferred_element_type=F32)


def spread(x, axes):
    copies = jnp.broadcast_to(x, (lax.axis_size(axes), *x.shape))
    return lax.all_to_all(copies, axes, split_axis=0, concat_axis=0, tiled=True)


def modulated(rows, gain, shift, scale):
    v = rows.astype(F32)
    v = v * lax.rsqrt(jnp.mean(v * v, axis=-1, keepdims=True) + EPS)
    return (v * gain * (1.0 + scale) + shift).astype(BF)


def rope_tables(start, count):
    quarter = HEAD_DIM // 4
    freq = THETA ** (-jnp.arange(quarter, dtype=F32) / quarter)
    rows = count // GRID_W
    row_angle = (start // GRID_W + jnp.arange(rows, dtype=jnp.int32)).astype(F32)[:, None] * freq
    col_angle = jnp.arange(GRID_W, dtype=jnp.int32).astype(F32)[:, None] * freq

    def table(fn, sign):
        r = fn(row_angle)
        c = fn(col_angle)
        r2 = jnp.broadcast_to(
            jnp.concatenate([sign * r, r], 1)[:, None], (rows, GRID_W, 2 * quarter)
        )
        c2 = jnp.broadcast_to(
            jnp.concatenate([sign * c, c], 1)[None], (rows, GRID_W, 2 * quarter)
        )
        return jnp.concatenate([r2, c2], -1).reshape(count, HEAD_DIM)

    return table(jnp.cos, 1.0), table(jnp.sin, -1.0)


def swapped(v):
    q = HEAD_DIM // 4
    return jnp.concatenate(
        [v[:, q : 2 * q], v[:, :q], v[:, 3 * q :], v[:, 2 * q : 3 * q]], axis=1
    )


def project_body(h_ref, w_ref, latent_ref, gate_ref, out_ref):
    acc = dot(h_ref[0], w_ref[0], ((1,), (0,)))
    for k in range(1, h_ref.shape[0]):
        acc = acc + dot(h_ref[k], w_ref[k], ((1,), (0,)))
    out_ref[...] = (latent_ref[...].astype(F32) + gate_ref[...] * acc).astype(BF)


def project(heads, weight, latent, gate):
    groups, rows, width = heads.shape
    cols = weight.shape[2]
    tile = min(512, cols)
    return pl.pallas_call(
        project_body,
        grid=(cols // tile,),
        in_specs=[
            pl.BlockSpec((groups, rows, width), lambda j: (0, 0, 0)),
            pl.BlockSpec((groups, width, tile), lambda j: (0, 0, j)),
            pl.BlockSpec((rows, tile), lambda j: (0, j)),
            pl.BlockSpec((1, tile), lambda j: (0, j)),
        ],
        out_specs=pl.BlockSpec((rows, tile), lambda j: (0, j)),
        out_shape=jax.ShapeDtypeStruct((rows, cols), BF),
        name="project",
    )(heads, weight, latent, gate)


def local(
    latent,
    context,
    condition,
    context_condition,
    shift_weight,
    scale_weight,
    mod_gate_weight,
    norm_gain,
    query_weight,
    key_weight,
    value_weight,
    gate_weight,
    forward_decay,
    backward_decay,
    out_weight,
):
    z, x = lax.axis_index("z"), lax.axis_index("x")
    nz, nx = lax.axis_size("z"), lax.axis_size("x")
    sp_index, sp_count = lax.axis_index(SP), nz * nx
    tokens = latent.shape[0]
    context_rows = context.shape[0]
    mod_rows = shift_weight.shape[0]

    full_weight = lax.all_gather(out_weight, TP, axis=0, tiled=False)

    activation = jax.nn.silu(jnp.stack([condition, context_condition]).astype(F32)).astype(BF)
    own = lax.dynamic_slice_in_dim(activation, sp_index * mod_rows, mod_rows, 1)
    partial = jnp.concatenate(
        [dot(own, m, ((1,), (0,))) for m in (shift_weight, scale_weight, mod_gate_weight)]
        + [jnp.zeros((2, shift_weight.shape[1]), F32)],
        axis=0,
    )
    summed = jnp.sum(spread(partial, SP), axis=0)
    modulation = spread(summed, TP)
    modulation = jnp.moveaxis(modulation, 0, 1).reshape(8, -1)
    gain = norm_gain.astype(F32)
    hidden = modulated(latent, gain, modulation[0], modulation[2])
    context_hidden = modulated(context, gain, modulation[1], modulation[3])

    stacked = jnp.concatenate([query_weight, key_weight, value_weight, gate_weight], axis=1)
    projected = dot(hidden, stacked, ((1,), (0,))).astype(BF)
    pairs = dot(context_hidden, stacked[:, HEAD_DIM : 3 * HEAD_DIM], ((1,), (0,))).astype(BF)
    context_pack = jnp.concatenate([pairs[:, :HEAD_DIM], pairs[:, HEAD_DIM:]], axis=0)

    cosine, sine = rope_tables(sp_index * tokens, tokens)
    scale = HEAD_DIM ** (-0.5)
    q0 = projected[:, :HEAD_DIM].astype(F32)
    k0 = projected[:, HEAD_DIM : 2 * HEAD_DIM].astype(F32)
    v = projected[:, 2 * HEAD_DIM : 3 * HEAD_DIM]
    out_gates = projected[:, 3 * HEAD_DIM :].astype(F32)
    q = q0 * cosine + swapped(q0) * sine
    k = (k0 * cosine + swapped(k0) * sine) * scale
    rate_f, rate_b = forward_decay[0], backward_decay[0]
    at = jnp.arange(tokens, dtype=F32)[:, None]
    state_f = dot((k * jnp.exp(-rate_f * (tokens - 1.0 - at))).astype(BF), v, ((0,), (0,)))
    state_b = dot((k * jnp.exp(-rate_b * at)).astype(BF), v, ((0,), (0,)))
    pack = jnp.concatenate([state_f.astype(BF), state_b.astype(BF), context_pack], axis=0)
    from_x = spread(pack, "x")

    span = float(tokens)
    xs = jnp.arange(nx, dtype=F32)
    xf = x.astype(F32)
    zf = z.astype(F32)
    sf = from_x[:, :HEAD_DIM].astype(F32)
    sb = from_x[:, HEAD_DIM : 2 * HEAD_DIM].astype(F32)
    context_group = from_x[:, 2 * HEAD_DIM :].reshape(-1, HEAD_DIM)

    def weighted(w, s):
        return jnp.sum(w[:, None, None] * s, axis=0)

    def power(rate, steps):
        return jnp.where(steps >= 0, jnp.exp(-rate * span * jnp.maximum(steps, 0.0)), 0.0)

    total_f = weighted(power(rate_f, nx - 1.0 - xs), sf).astype(BF)
    total_b = weighted(power(rate_b, xs), sb).astype(BF)
    before_x = weighted(power(rate_f, xf - 1.0 - xs), sf)
    after_x = weighted(power(rate_b, xs - xf - 1.0), sb)
    zs = jnp.arange(nz, dtype=jnp.int32)
    chosen = jnp.where((zs > z)[:, None, None], total_f[None], total_b[None])
    message = jnp.concatenate(
        [chosen, jnp.broadcast_to(context_group[None], (nz, *context_group.shape))], axis=1
    )
    from_z = lax.all_to_all(message, "z", split_axis=0, concat_axis=0, tiled=True)

    gap = at - jnp.arange(tokens, dtype=F32)[None, :]
    mixing = jnp.exp(jnp.where(gap >= 0, -rate_f * gap, rate_b * gap)) + jnp.where(
        gap == 0, 1.0, 0.0
    )
    scores = (dot(q.astype(BF), k.astype(BF), ((1,), (1,))) * mixing).astype(BF)
    local_out = dot(scores, v, ((1,), (0,)))

    zsf = zs.astype(F32)
    sz = from_z[:, :HEAD_DIM].astype(F32)
    cz = from_z[:, HEAD_DIM:].reshape(sp_count, 2, context_rows, HEAD_DIM)
    ck = cz[:, 0].reshape(-1, HEAD_DIM).astype(F32) * (scale * CONTEXT_LIFT)
    cv = cz[:, 1].reshape(-1, HEAD_DIM)
    total = context_rows * sp_count
    cat = jnp.arange(total, dtype=F32)[:, None]
    context_f = dot((ck * jnp.exp(-rate_f * (total - 1.0 - cat))).astype(BF), cv, ((0,), (0,)))
    context_b = dot((ck * jnp.exp(-rate_b * cat)).astype(BF), cv, ((0,), (0,)))
    block = sp_index.astype(F32)
    incoming_f = (
        before_x
        + weighted(power(rate_f, xf) * power(rate_f, nx * (zf - 1.0 - zsf)), sz)
        + power(rate_f, block) * context_f
    )
    incoming_b = (
        after_x
        + weighted(power(rate_b, nx - 1.0 - xf) * power(rate_b, nx * (zsf - zf - 1.0)), sz)
        + power(rate_b, sp_count - 1.0 - block) * context_b
    )
    read_f = dot(
        (q * jnp.exp(-rate_f * (at + 1.0))).astype(BF), incoming_f.astype(BF), ((1,), (0,))
    )
    read_b = dot(
        (q * jnp.exp(-rate_b * (tokens - at))).astype(BF), incoming_b.astype(BF), ((1,), (0,))
    )
    retained = local_out + read_f + read_b
    retained = retained * lax.rsqrt(jnp.mean(retained * retained, axis=-1, keepdims=True) + EPS)
    heads = (jax.nn.silu(out_gates) * retained).astype(BF)
    all_heads = lax.all_gather(heads, TP, axis=0, tiled=False)
    return project(all_heads, full_weight, latent, modulation[4:5])


def solution(mesh):
    torus = Mesh(mesh.devices.reshape(8, 4, 8, 2), ("z", "x", "y", "c"))
    rows, cols = P(SP, None), P(None, TP)
    both = P(SP, TP)
    in_specs = (
        (rows, rows, P(), P(), both, both, both, P(), cols, cols, cols, cols)
        + (P(TP), P(TP), P(TP, None))
    )
    return jax.shard_map(local, mesh=torus, in_specs=in_specs, out_specs=rows, check_vma=False)
```

time: 354 us -> 205 us (0.58)
  blocking collectives: 136 us -> 0 us
  matrix products: 30.2 us -> 8.78 us
  starting transfers between devices: 13.8 us -> 29.9 us
  Pallas kernels: 0 us -> 12.7 us
  waiting for transfers between devices: 132 us -> 122 us
  between operations: 24.2 us -> 15.3 us
    all_gather x0 -> x2, waiting for transfers between devices: none -> 85.8 us  [the longest x1 55.3 us: local(): full_weight = lax.all_gather(out_weight, TP, axis=0, tiled=False)]
    all_gather x5 -> x0, blocking collectives: 78.6 us -> none  [the longest x4 59 us: all_in_one(): both, at, found = (lax.all_gather(jnp.concatenate(lines), axis), 0, {})]
    reduce_scatter x1 -> x0, waiting for transfers between devices: 66.3 us -> none  [local(): lax.psum_scatter(jnp.dot(heads_out, out_weight, preferred_element_type=jn...]
    psum x1 -> x0, waiting for transfers between devices: 61.9 us -> none  [in_one(): total = lax.psum(ravelled, axis)]
    all_to_all x1 -> x0, blocking collectives: 57.7 us -> none  [sent_to_all(): return lax.all_to_all(copies, axis, split_axis=0, concat_axis=0, tiled=True)]
    all_to_all x1 -> x4, waiting for transfers between devices: 3.64 us -> 35.8 us  [the longest x3 18.2 us: spread(): return lax.all_to_all(copies, axes, split_axis=0, concat_axis=0, tiled=True)]
    dot_general x14 -> x10, matrix products: 30.2 us -> 8.78 us  [dot(): return lax.dot_general(a, b, (dims, ((), ())), preferred_element_type=F32)]
    all_to_all x1 -> x4, starting transfers between devices: 13.7 us -> 29.8 us  [the longest x3 26.3 us: spread(): return lax.all_to_all(copies, axes, split_axis=0, concat_axis=0, tiled=True)]
  transfers between devices with their start and end apart: 3 -> 6, of which waited for: 3 -> 6; matrix products, arithmetic and copies ran while one was open for 5% -> 4% of each run, Pallas kernels for 0% -> 0%
where the time goes in v1:
time: 205 us; the launch traced here: 204 us
  waiting for transfers between devices  122 us (60%)
  starting transfers between devices  29.9 us (15%)
  between operations  15.3 us (7%)
  Pallas kernels  12.7 us (6%)
  matrix products  8.78 us (4%)
  local copies, waits for them, and re-layouts  8.07 us (4%)
  other arithmetic  7.06 us (3%)
    all_gather x1, waiting for transfers between devices, local(): full_weight = lax.all_gather(out_weight, TP, axis=0, tiled=False)  55.3 us
    all_gather x1, waiting for transfers between devices, local(): all_heads = lax.all_gather(heads, TP, axis=0, tiled=False)  30.5 us
    all_to_all x3, starting transfers between devices, spread(): return lax.all_to_all(copies, axes, split_axis=0, concat_axis=0, tiled=True)  26.3 us
    all_to_all x3, waiting for transfers between devices, spread(): return lax.all_to_all(copies, axes, split_axis=0, concat_axis=0, tiled=True)  18.2 us
    all_to_all x1, waiting for transfers between devices, local(): lax.all_to_all(message, 'z', split_axis=0, concat_axis=0, tiled=True)  17.5 us
    pallas_call x1, Pallas kernels, project(): pl.pallas_call(project_body, grid=(cols // tile,), in_specs=[pl.BlockSpec...  12.7 us
    dot_general x10, matrix products, dot(): return lax.dot_general(a, b, (dims, ((), ())), preferred_element_type=F32)  8.78 us
  transfers between devices with their start and end apart: 6, of which 6 were waited for; matrix products, arithmetic and copies ran while one was open for 4% of the time, Pallas kernels for 0%

profile of v1, /device:TPU:1, one launch (start us, length us, event | category | flops | bytes accessed | tf_op | source)
XLA Modules:
  0.0 204.0 jit_solution(698090426259455033)
XLA Ops:
  6.5 0.7 stack.9
  7.3 0.7 stack.10
  8.0 0.2 fusion.117
  8.2 0.9 fusion.115
  9.1 0.9 fusion.119
  10.0 0.1 pad.35.clone
  10.1 0.1 maximum_maximum_fusion
  10.2 0.7 broadcast_in_dim.47
  10.9 13.7 %all-to-all-start = ((f32[32,8,128]{2,1,0:T(8,128)}), f32[32,8,128]{2,1,0:T(8,128)S(1)}, u32[]{:S(2)}, u32[]{:S(2)}) async-start(f32[32,8,128]{2,1,0:T(8,128)} %broadcast_in_dim.47), calls=%async_computation | async-start | bytes 262144 | tf_op jit(solution)/shard_map/all_to_all | solution.py:26
  25.3 1.0 fusion.67
  26.3 2.2 %fusion = f32[512]{0:T(512)S(1)} fusion(bf16[512,2048]{1,0:T(8,128)(2,1)} %latent_ref.1), kind=kLoop, calls=%fused_computation.2 | loop fusion | flops 3145216 | bytes 2099200 | tf_op jit(solution)/shard_map/reduce_sum | solution.py:31
  28.5 0.1 multiply_cosine_fusion.1
  28.6 0.2 multiply_cosine_fusion
  28.8 0.1 pad_maximum_fusion.6
  28.9 0.1 pad_maximum_fusion.4
  29.0 0.1 pad_maximum_fusion.1
  29.2 0.1 pad_maximum_fusion.2
  30.1 3.9 %all-to-all-done = f32[32,8,128]{2,1,0:T(8,128)S(1)} async-done(((f32[32,8,128]{2,1,0:T(8,128)}), f32[32,8,128]{2,1,0:T(8,128)S(1)}, u32[]{:S(2)}, u32[]{:S(2)}) %all-to-all-start) | async-done | bytes 131104 | tf_op jit(solution)/shard_map/all_to_all | solution.py:26
  34.0 0.6 broadcast_in_dim.48
  34.6 9.2 %all-to-all-start.1 = ((f32[16,8,128]{2,1,0:T(8,128)}), f32[16,8,128]{2,1,0:T(8,128)S(1)}, u32[]{:S(2)}, u32[]{:S(2)}) async-start(f32[16,8,128]{2,1,0:T(8,128)} %broadcast_in_dim.48), calls=%async_computation.1 | async-start | bytes 131072 | tf_op jit(solution)/shard_map/all_to_all | solution.py:26
  43.8 0.1 copy.33
  43.9 0.1 copy.34
  44.1 7.4 %all-to-all-done.1 = f32[16,8,128]{2,1,0:T(8,128)S(1)} async-done(((f32[16,8,128]{2,1,0:T(8,128)}), f32[16,8,128]{2,1,0:T(8,128)S(1)}, u32[]{:S(2)}, u32[]{:S(2)}) %all-to-all-start.1) | async-done | bytes 65568 | tf_op jit(solution)/shard_map/all_to_all | solution.py:26
  51.5 0.6 slice_bitcast_fusion.5
  52.2 1.5 convolution_convert_fusion.2
  53.7 3.0 %fusion.19 = bf16[512,512]{0,1:T(8,128)(2,1)S(1)} fusion(bf16[2048,128]{1,0:T(8,128)(2,1)} %param.26, bf16[2048,128]{1,0:T(8,128)(2,1)} %param.25, bf16[2048,128]{1,0:T(8,128)(2,1)} %param.24, bf16[2048,128]{1,0:T(8,128)(2,1)} %param.23, bf16[512,2048]{1,0:T(8,128)(2,1)S(1)} %copy-done.1, f32[2048]{0:T(1024)S(1)} %bitcast.64, f32[2048]{0:T(1024)S(1)} %bitcast.65, ...), kind=kOutput, calls=%fused_computation.21 | convolution fusion | flops 1088684032 | bytes 4745216 | tf_op jit(solution)/shard_map/dot_general | solution.py:21
  56.7 0.1 slice_convert_fusion
  56.8 0.1 fusion.65
  57.0 0.2 convolution_convert_fusion
  57.1 0.2 convolution_convert_fusion.1
  57.4 0.8 broadcast_in_dim.63
  58.1 3.5 %all-to-all-start.2 = ((bf16[4,288,128]{2,1,0:T(8,128)(2,1)}), bf16[4,288,128]{2,1,0:T(8,128)(2,1)S(1)}, u32[]{:S(2)}, u32[]{:S(2)}) async-start(bf16[4,288,128]{2,1,0:T(8,128)(2,1)} %broadcast_in_dim.63), calls=%async_computation.2 | async-start | bytes 589824 | tf_op jit(solution)/shard_map/all_to_all | solution.py:26
  61.6 6.9 %all-to-all-done.2 = bf16[4,288,128]{2,1,0:T(8,128)(2,1)S(1)} async-done(((bf16[4,288,128]{2,1,0:T(8,128)(2,1)}), bf16[4,288,128]{2,1,0:T(8,128)(2,1)S(1)}, u32[]{:S(2)}, u32[]{:S(2)}) %all-to-all-start.2) | async-done | bytes 294944 | tf_op jit(solution)/shard_map/all_to_all | solution.py:26
  68.5 0.2 fusion.58
  68.7 0.1 broadcast_select_fusion
  68.8 0.8 pad_maximum_fusion
  69.7 3.5 %all-to-all-start.3 = ((bf16[8,256,128]{2,1,0:T(8,128)(2,1)}), bf16[8,256,128]{2,1,0:T(8,128)(2,1)S(1)}, u32[]{:S(2)}, u32[]{:S(2)}) async-start(bf16[8,256,128]{2,1,0:T(8,128)(2,1)} %pad_maximum_fusion), calls=%async_computation.3 | async-start | bytes 1048576 | tf_op jit(solution)/shard_map/all_to_all | solution.py:172
  73.5 17.5 %all-to-all-done.3 = bf16[8,256,128]{2,1,0:T(8,128)(2,1)S(1)} async-done(((bf16[8,256,128]{2,1,0:T(8,128)(2,1)}), bf16[8,256,128]{2,1,0:T(8,128)(2,1)S(1)}, u32[]{:S(2)}, u32[]{:S(2)}) %all-to-all-start.3) | async-done | bytes 524320 | tf_op jit(solution)/shard_map/all_to_all | solution.py:172
  91.1 0.2 fusion.48
  91.3 0.5 fusion.33
  91.8 0.5 fusion.34
  92.3 0.8 multiply_reduce_fusion
  93.1 0.7 fusion.66
  94.0 0.7 all-gather.7.cloned.1.call-update
  94.7 30.5 %all-gather.5.cloned.1.call-done = bf16[8192,128]{0,1:T(8,128)(2,1)} async-done(((bf16[512,128]{0,1:T(8,128)(2,1)}), bf16[8192,128]{0,1:T(8,128)(2,1)}) %all-gather.5.cloned.1.call-update) | async-done | bytes 2097168 | tf_op jit(solution)/shard_map/all_gather | solution.py:210
  125.2 4.0 %copy.38 = bf16[8192,128]{1,0:T(8,128)(2,1)} copy(bf16[8192,128]{0,1:T(8,128)(2,1)} %all-gather.5.cloned.1.call-done) | data formatting | bytes 4194304 | tf_op jit(solution)/shard_map/all_gather | solution.py:210
  129.2 55.3 %all-gather.7.cloned.1.call-done = bf16[2048,2048]{1,0:T(8,128)(2,1)} async-done(((bf16[128,2048]{1,0:T(8,128)(2,1)}), bf16[2048,2048]{1,0:T(8,128)(2,1)}) %all-gather.7.cloned.1.call-update) | async-done | bytes 8388624 | tf_op jit(solution)/shard_map/all_gather | solution.py:113
  184.5 12.7 %project.1 = bf16[512,2048]{1,0:T(8,128)(2,1)} custom-call(bf16[16,512,128]{2,1,0:T(8,128)(2,1)} %bitcast.56, bf16[16,128,2048]{2,1,0:T(8,128)(2,1)} %bitcast.57, bf16[512,2048]{1,0:T(8,128)(2,1)} %latent_ref.1, f32[1,2048]{1,0:T(1,128)} %get-tuple-element.23.gate_ref), custom_call_target="tpu_custom_call" | custom-call | tf_op jit(solution)/shard_map/project/pallas_call | solution.py:74
  (41 shorter events, 0.5 us)
Async XLA Ops:
  6.5 1.5 copy-start
  6.5 45.6 %copy-start.2 = (bf16[16,2048]{1,0:T(8,128)(2,1)S(1)}, bf16[16,2048]{1,0:T(8,128)(2,1)}, u32[]{:S(2)}) copy-start(bf16[16,2048]{1,0:T(8,128)(2,1)} %param.16) | copy-start | bytes 196612
  6.5 37.3 %copy-start.3 = (bf16[2048]{0:T(1024)(128)(2,1)S(1)}, bf16[2048]{0:T(1024)(128)(2,1)}, u32[]{:S(2)}) copy-start(bf16[2048]{0:T(1024)(128)(2,1)} %param.22) | copy-start | bytes 12292
  10.9 23.1 %all-to-all-start = ((f32[32,8,128]{2,1,0:T(8,128)}), f32[32,8,128]{2,1,0:T(8,128)S(1)}, u32[]{:S(2)}, u32[]{:S(2)}) async-start(f32[32,8,128]{2,1,0:T(8,128)} %broadcast_in_dim.47), calls=%async_computation | async-start | bytes 262144 | tf_op jit(solution)/shard_map/all_to_all | solution.py:26
  26.3 27.4 %copy-start.1 = (bf16[512,2048]{1,0:T(8,128)(2,1)S(1)}, bf16[512,2048]{1,0:T(8,128)(2,1)}, u32[]{:S(2)}) copy-start(bf16[512,2048]{1,0:T(8,128)(2,1)} %latent_ref.1) | copy-start | bytes 6291460
  34.6 16.9 %all-to-all-start.1 = ((f32[16,8,128]{2,1,0:T(8,128)}), f32[16,8,128]{2,1,0:T(8,128)S(1)}, u32[]{:S(2)}, u32[]{:S(2)}) async-start(f32[16,8,128]{2,1,0:T(8,128)} %broadcast_in_dim.48), calls=%async_computation.1 | async-start | bytes 131072 | tf_op jit(solution)/shard_map/all_to_all | solution.py:26
  58.1 10.4 %all-to-all-start.2 = ((bf16[4,288,128]{2,1,0:T(8,128)(2,1)}), bf16[4,288,128]{2,1,0:T(8,128)(2,1)S(1)}, u32[]{:S(2)}, u32[]{:S(2)}) async-start(bf16[4,288,128]{2,1,0:T(8,128)(2,1)} %broadcast_in_dim.63), calls=%async_computation.2 | async-start | bytes 589824 | tf_op jit(solution)/shard_map/all_to_all | solution.py:26
  69.7 21.4 %all-to-all-start.3 = ((bf16[8,256,128]{2,1,0:T(8,128)(2,1)}), bf16[8,256,128]{2,1,0:T(8,128)(2,1)S(1)}, u32[]{:S(2)}, u32[]{:S(2)}) async-start(bf16[8,256,128]{2,1,0:T(8,128)(2,1)} %pad_maximum_fusion), calls=%async_computation.3 | async-start | bytes 1048576 | tf_op jit(solution)/shard_map/all_to_all | solution.py:172
  73.2 52.0 %all-gather.5.cloned.1.call-start = ((), (), s32[]{:S(2)}) async-start(), calls=%async_computation.4 | async-start | bytes 2228224 | tf_op jit(solution)/shard_map/all_gather | solution.py:210
  93.9 90.5 %all-gather.7.cloned.1.call-start = ((), (), s32[]{:S(2)}) async-start(), calls=%async_computation.5 | async-start | bytes 8912896 | tf_op jit(solution)/shard_map/all_gather | solution.py:113
Sparse Core Ops, SparseCore 0:
  94.0 31.0 all-gather.4
  127.3 57.1 all-gather.6

commit v2 on v1

v2 whole, which is shorter than its diff:
```python
import jax
import jax.numpy as jnp
from jax import lax
from jax.experimental import pallas as pl
from jax.experimental.pallas import tpu as pltpu
from jax.sharding import Mesh
from jax.sharding import PartitionSpec as P

HEAD_DIM = 128
GRID_W = 64
SP = ("z", "x")
TP = ("y", "c")
EPS = 1e-06
THETA = 10000.0
CONTEXT_LIFT = 3.0
BF = jnp.bfloat16
F32 = jnp.float32


def dot(a, b, dims):
    return lax.dot_general(a, b, (dims, ((), ())), preferred_element_type=F32)


def rope_tables(start, count):
    quarter = HEAD_DIM // 4
    freq = THETA ** (-jnp.arange(quarter, dtype=F32) / quarter)
    rows = count // GRID_W
    row_angle = (start // GRID_W + jnp.arange(rows, dtype=jnp.int32)).astype(F32)[:, None] * freq
    col_angle = jnp.arange(GRID_W, dtype=jnp.int32).astype(F32)[:, None] * freq

    def table(fn, sign):
        r = fn(row_angle)
        c = fn(col_angle)
        r2 = jnp.broadcast_to(
            jnp.concatenate([sign * r, r], 1)[:, None], (rows, GRID_W, 2 * quarter)
        )
        c2 = jnp.broadcast_to(
            jnp.concatenate([sign * c, c], 1)[None], (rows, GRID_W, 2 * quarter)
        )
        return jnp.concatenate([r2, c2], -1).reshape(count, HEAD_DIM)

    return table(jnp.cos, 1.0), table(jnp.sin, -1.0)


def roll_pairs(v):
    q = HEAD_DIM // 4
    lane = lax.broadcasted_iota(jnp.int32, v.shape, 1)
    low = (lane % (2 * q)) < q
    return jnp.where(low, pltpu.roll(v, HEAD_DIM - q, 1), pltpu.roll(v, q, 1))


def side_by_side(ref, row):
    return jnp.concatenate([ref[k, row : row + 1, :] for k in range(ref.shape[0])], axis=1)


def partial_body(act_ref, at_ref, shift_ref, scale_ref, gate_ref, out_ref):
    own = act_ref[pl.ds(at_ref[0], 1)][0].astype(F32)
    own = (own * (1.0 / (1.0 + jnp.exp(-own)))).astype(BF)
    parts = [dot(own, m[...], ((1,), (0,))) for m in (shift_ref, scale_ref, gate_ref)]
    both = jnp.concatenate(parts + [jnp.zeros_like(parts[0])], axis=0)
    out_ref[...] = jnp.broadcast_to(both[None], out_ref.shape)


def sum_body(in_ref, out_ref):
    total = in_ref[0]
    for k in range(1, in_ref.shape[0]):
        total = total + in_ref[k]
    out_ref[...] = jnp.broadcast_to(total[None], out_ref.shape)


def normed(rows, factor, shift):
    v = rows.astype(F32)
    r = lax.rsqrt(jnp.mean(v * v, axis=-1, keepdims=True) + EPS)
    return (v * r * factor + shift).astype(BF)


def front_body(
    latent_ref,
    context_ref,
    mod_ref,
    gain_ref,
    weight_ref,
    cos_ref,
    sin_ref,
    par_ref,
    message_ref,
    q_ref,
    g_ref,
    local_ref,
    state_ref,
    modgate_ref,
    k_scr,
    v_scr,
):
    step, steps = pl.program_id(0), pl.num_programs(0)
    tile = latent_ref.shape[0]
    tokens = k_scr.shape[0]
    scale = HEAD_DIM ** (-0.5)
    gain = gain_ref[...].astype(F32)
    h = normed(
        latent_ref[...], gain * (1.0 + side_by_side(mod_ref, 2)), side_by_side(mod_ref, 0)
    )
    proj = dot(h, weight_ref[...], ((1,), (0,))).astype(BF)
    at = pl.ds(pl.multiple_of(step * tile, tile), tile)
    cosine, sine = cos_ref[at, :], sin_ref[at, :]
    q0 = proj[:, :HEAD_DIM].astype(F32)
    k0 = proj[:, HEAD_DIM : 2 * HEAD_DIM].astype(F32)
    q_ref[at, :] = q0 * cosine + roll_pairs(q0) * sine
    k_scr[at, :] = (k0 * cosine + roll_pairs(k0) * sine) * scale
    v_scr[at, :] = proj[:, 2 * HEAD_DIM : 3 * HEAD_DIM]
    g_ref[at, :] = proj[:, 3 * HEAD_DIM :]

    @pl.when(step == steps - 1)
    def _():
        rate_f, rate_b, zf = par_ref[0:1, :], par_ref[1:2, :], par_ref[2:3, :]
        hc = normed(
            context_ref[...], gain * (1.0 + side_by_side(mod_ref, 3)), side_by_side(mod_ref, 1)
        )
        pairs = dot(hc, weight_ref[:, HEAD_DIM : 3 * HEAD_DIM], ((1,), (0,))).astype(BF)
        modgate_ref[...] = side_by_side(mod_ref, 4)
        k = k_scr[...]
        v = v_scr[...]
        row = lax.broadcasted_iota(jnp.int32, (tokens, HEAD_DIM), 0).astype(F32)
        state_f = dot((k * jnp.exp(-rate_f * (tokens - 1.0 - row))).astype(BF), v, ((0,), (0,)))
        state_b = dot((k * jnp.exp(-rate_b * row)).astype(BF), v, ((0,), (0,)))
        state_ref[0] = state_f
        state_ref[1] = state_b
        rows = context_ref.shape[0]
        for n in range(message_ref.shape[0]):
            message_ref[n, :HEAD_DIM, :] = jnp.where(zf < n, state_f, state_b).astype(BF)
            message_ref[n, HEAD_DIM : HEAD_DIM + rows, :] = pairs[:, :HEAD_DIM]
            message_ref[n, HEAD_DIM + rows :, :] = pairs[:, HEAD_DIM:]
        kb = k.astype(BF)
        f1, b1 = rate_f[:, :1], rate_b[:, :1]
        for n in range(tokens // tile):
            qb = q_ref[n * tile : (n + 1) * tile, :].astype(BF)
            gap = (
                lax.broadcasted_iota(jnp.int32, (tile, tokens), 0)
                + n * tile
                - lax.broadcasted_iota(jnp.int32, (tile, tokens), 1)
            ).astype(F32)
            mixing = jnp.exp(jnp.where(gap >= 0, -f1 * gap, b1 * gap)) * jnp.where(
                gap == 0, 2.0, 1.0
            )
            scores = (dot(qb, kb, ((1,), (1,))) * mixing).astype(BF)
            local_ref[n * tile : (n + 1) * tile, :] = dot(scores, v, ((1,), (0,)))


def middle_body(from_ref, state_ref, par_ref, message_ref, *, span, context_rows):
    nz, nx = from_ref.shape[0], message_ref.shape[0]
    rate_f, rate_b, zf, xf = (par_ref[k : k + 1, :] for k in range(4))

    def power(rate, blocks):
        kept = jnp.exp(-rate * (span * jnp.maximum(blocks, 0.0)))
        return jnp.where(blocks >= 0, kept, 0.0)

    sum_f = jnp.zeros((HEAD_DIM, HEAD_DIM), F32)
    sum_b = jnp.zeros((HEAD_DIM, HEAD_DIM), F32)
    for n in range(nz):
        s = from_ref[n, :HEAD_DIM, :].astype(F32)
        sum_f = sum_f + power(rate_f, nx * (zf - 1.0 - n)) * s
        sum_b = sum_b + power(rate_b, nx * (n - zf - 1.0)) * s
    total = float(context_rows * nz * nx)
    keys, values, at = [], [], []
    for n in range(nz):
        keys.append(from_ref[n, HEAD_DIM : HEAD_DIM + context_rows, :].astype(F32))
        values.append(from_ref[n, HEAD_DIM + context_rows :, :])
        at.append(
            lax.broadcasted_iota(jnp.int32, (context_rows, HEAD_DIM), 0).astype(F32)
            + context_rows * (nx * n + xf)
        )
    ck = jnp.concatenate(keys, 0) * (HEAD_DIM ** (-0.5) * CONTEXT_LIFT)
    cv = jnp.concatenate(values, 0)
    at = jnp.concatenate(at, 0)
    context_f = dot((ck * jnp.exp(-rate_f * (total - 1.0 - at))).astype(BF), cv, ((0,), (0,)))
    context_b = dot((ck * jnp.exp(-rate_b * at)).astype(BF), cv, ((0,), (0,)))
    own_f, own_b = state_ref[0], state_ref[1]
    for n in range(nx):
        message_ref[n, :HEAD_DIM, :] = (
            power(rate_f, nx - 1.0 + n - xf) * sum_f
            + power(rate_f, n - 1.0 - xf) * own_f
            + power(rate_f, nx * zf + n) * context_f
        ).astype(BF)
        message_ref[n, HEAD_DIM:, :] = (
            power(rate_b, nx - 1.0 + xf - n) * sum_b
            + power(rate_b, xf - n - 1.0) * own_b
            + power(rate_b, nx * nz - 1.0 - nx * zf - n) * context_b
        ).astype(BF)


def finish_body(from_ref, q_ref, g_ref, local_ref, par_ref, out_ref):
    tokens = q_ref.shape[0]
    rate_f, rate_b = par_ref[0:1, :], par_ref[1:2, :]
    incoming = from_ref[0].astype(F32)
    for n in range(1, from_ref.shape[0]):
        incoming = incoming + from_ref[n].astype(F32)
    row = lax.broadcasted_iota(jnp.int32, (tokens, HEAD_DIM), 0).astype(F32)
    q = q_ref[...]
    reads = jnp.concatenate(
        [
            (q * jnp.exp(-rate_f * (row + 1.0))).astype(BF),
            (q * jnp.exp(-rate_b * (tokens - row))).astype(BF),
        ],
        axis=1,
    )
    kept = local_ref[...] + dot(reads, incoming.astype(BF), ((1,), (0,)))
    kept = kept * lax.rsqrt(jnp.mean(kept * kept, axis=-1, keepdims=True) + EPS)
    g = g_ref[...].astype(F32)
    out_ref[...] = (g * (1.0 / (1.0 + jnp.exp(-g))) * kept).astype(BF)


def project_body(h_ref, w_ref, latent_ref, gate_ref, out_ref, h_scr):
    groups, _, width = h_ref.shape

    @pl.when(pl.program_id(0) == 0)
    def _():
        for k in range(groups):
            h_scr[:, k * width : (k + 1) * width] = h_ref[k]

    acc = dot(h_scr[...], w_ref[...], ((1,), (0,)))
    out_ref[...] = (latent_ref[...].astype(F32) + gate_ref[...] * acc).astype(BF)


def project(heads, weight, latent, gate):
    groups, rows, width = heads.shape
    depth, cols = weight.shape
    tile = 512
    return pl.pallas_call(
        project_body,
        grid=(cols // tile,),
        in_specs=[
            pl.BlockSpec((groups, rows, width), lambda j: (0, 0, 0)),
            pl.BlockSpec((depth, tile), lambda j: (0, j)),
            pl.BlockSpec((rows, tile), lambda j: (0, j)),
            pl.BlockSpec((1, tile), lambda j: (0, j)),
        ],
        out_specs=pl.BlockSpec((rows, tile), lambda j: (0, j)),
        out_shape=jax.ShapeDtypeStruct((rows, cols), BF),
        scratch_shapes=[pltpu.VMEM((rows, depth), BF)],
        name="project",
    )(heads, weight, latent, gate)


def whole(body, shapes, name, **options):
    return pl.pallas_call(body, out_shape=shapes, name=name, **options)


def local(
    latent,
    context,
    condition,
    context_condition,
    shift_weight,
    scale_weight,
    mod_gate_weight,
    norm_gain,
    query_weight,
    key_weight,
    value_weight,
    gate_weight,
    forward_decay,
    backward_decay,
    out_weight,
):
    z, x = lax.axis_index("z"), lax.axis_index("x")
    nz, nx, nt = lax.axis_size("z"), lax.axis_size("x"), lax.axis_size(TP)
    sp_index, sp_count = lax.axis_index(SP), nz * nx
    tokens, model = latent.shape
    context_rows = context.shape[0]
    mod_rows, mod_cols = shift_weight.shape

    full_weight = lax.all_gather(out_weight, TP, axis=0, tiled=True)

    conditions = jnp.stack([condition, context_condition])
    conditions = jnp.swapaxes(conditions.reshape(2, sp_count, mod_rows), 0, 1)
    memory = pltpu.MemorySpace
    partial = whole(
        partial_body,
        jax.ShapeDtypeStruct((sp_count, 8, mod_cols), F32),
        "partial",
        in_specs=[
            pl.BlockSpec(memory_space=memory.VMEM),
            pl.BlockSpec(memory_space=memory.SMEM),
        ]
        + [pl.BlockSpec(memory_space=memory.VMEM)] * 3,
    )(conditions, sp_index.reshape(1), shift_weight, scale_weight, mod_gate_weight)

    stacked = jnp.concatenate([query_weight, key_weight, value_weight, gate_weight], axis=1)
    cosine, sine = rope_tables(sp_index * tokens, tokens)
    numbers = jnp.stack(
        [forward_decay[0], backward_decay[0], z.astype(F32), x.astype(F32)]
        + [jnp.zeros((), F32)] * 4
    )
    par = jnp.broadcast_to(numbers[:, None], (8, HEAD_DIM))
    partial, stacked, cosine, sine, par, gain = lax.optimization_barrier(
        (partial, stacked, cosine, sine, par, norm_gain[None])
    )

    gathered = lax.all_to_all(partial, SP, split_axis=0, concat_axis=0, tiled=True)
    summed = whole(sum_body, jax.ShapeDtypeStruct((nt, 8, mod_cols), F32), "sum")(gathered)
    modulation = lax.all_to_all(summed, TP, split_axis=0, concat_axis=0, tiled=True)

    tile = 128
    pinned = lambda *shape: pl.BlockSpec(shape, lambda i: (0,) * len(shape))
    message_rows = HEAD_DIM + 2 * context_rows
    message, q, g, local_out, states, mod_gate = pl.pallas_call(
        front_body,
        grid=(tokens // tile,),
        in_specs=[
            pl.BlockSpec((tile, model), lambda i: (i, 0)),
            pinned(*context.shape),
            pinned(nt, 8, mod_cols),
            pinned(1, model),
            pinned(model, 4 * HEAD_DIM),
            pinned(tokens, HEAD_DIM),
            pinned(tokens, HEAD_DIM),
            pinned(8, HEAD_DIM),
        ],
        out_specs=[
            pinned(nz, message_rows, HEAD_DIM),
            pinned(tokens, HEAD_DIM),
            pinned(tokens, HEAD_DIM),
            pinned(tokens, HEAD_DIM),
            pinned(2, HEAD_DIM, HEAD_DIM),
            pinned(1, model),
        ],
        out_shape=[
            jax.ShapeDtypeStruct((nz, message_rows, HEAD_DIM), BF),
            jax.ShapeDtypeStruct((tokens, HEAD_DIM), F32),
            jax.ShapeDtypeStruct((tokens, HEAD_DIM), BF),
            jax.ShapeDtypeStruct((tokens, HEAD_DIM), F32),
            jax.ShapeDtypeStruct((2, HEAD_DIM, HEAD_DIM), F32),
            jax.ShapeDtypeStruct((1, model), F32),
        ],
        scratch_shapes=[
            pltpu.VMEM((tokens, HEAD_DIM), F32),
            pltpu.VMEM((tokens, HEAD_DIM), BF),
        ],
        name="front",
    )(latent, context, modulation, gain, stacked, cosine, sine, par)
    from_z = lax.all_to_all(message, "z", split_axis=0, concat_axis=0, tiled=True)
    message = whole(
        lambda *refs: middle_body(*refs, span=float(tokens), context_rows=context_rows),
        jax.ShapeDtypeStruct((nx, 2 * HEAD_DIM, HEAD_DIM), BF),
        "middle",
    )(from_z, states, par)
    from_x = lax.all_to_all(message, "x", split_axis=0, concat_axis=0, tiled=True)
    heads = whole(finish_body, jax.ShapeDtypeStruct((tokens, HEAD_DIM), BF), "finish")(
        from_x, q, g, local_out, par
    )
    heads, full_weight = lax.optimization_barrier((heads, full_weight))
    all_heads = lax.all_gather(heads, TP, axis=0, tiled=False)
    return project(all_heads, full_weight, latent, mod_gate)


def solution(mesh):
    torus = Mesh(mesh.devices.reshape(8, 4, 8, 2), ("z", "x", "y", "c"))
    rows, cols = P(SP, None), P(None, TP)
    both = P(SP, TP)
    in_specs = (
        (rows, rows, P(), P(), both, both, both, P(), cols, cols, cols, cols)
        + (P(TP), P(TP), P(TP, None))
    )
    return jax.shard_map(local, mesh=torus, in_specs=in_specs, out_specs=rows, check_vma=False)
```

time: 205 us -> 150 us (0.73)
  waiting for transfers between devices: 122 us -> 33.2 us
  blocking collectives: 0 us -> 69.2 us
  starting transfers between devices: 29.9 us -> 0.07 us
  Pallas kernels: 12.7 us -> 24.4 us
  matrix products: 8.78 us -> 0 us
  local copies, waits for them, and re-layouts: 8.07 us -> 3.66 us
  other arithmetic: 7.06 us -> 4.42 us
    all_to_all x0 -> x4, blocking collectives: none -> 69.2 us  [the longest x1 22.9 us: local(): lax.all_to_all(partial, SP, split_axis=0, concat_axis=0, tiled=True)]
    all_gather x1, waiting for transfers between devices: 55.3 us -> 0.01 us  [local(): full_weight = lax.all_gather(out_weight, TP, axis=0, tiled=True)]
    all_to_all x4 -> x0, waiting for transfers between devices: 35.8 us -> none  [the longest x3 18.2 us: spread(): return lax.all_to_all(copies, axes, split_axis=0, concat_axis=0, tiled=True)]
    all_to_all x4 -> x0, starting transfers between devices: 29.8 us -> none  [the longest x3 26.3 us: spread(): return lax.all_to_all(copies, axes, split_axis=0, concat_axis=0, tiled=True)]
    pallas_call x0 -> x5, Pallas kernels: none -> 14.6 us  [the longest x1 7.17 us: local(): pl.pallas_call(front_body, grid=(tokens // tile,), in_specs=[pl.BlockSpec...]
    dot_general x10 -> x0, matrix products: 8.78 us -> none  [dot(): return lax.dot_general(a, b, (dims, ((), ())), preferred_element_type=F32)]
    all_gather x1 -> x0, local copies, waits for them, and re-layouts: 4.04 us -> none  [local(): all_heads = lax.all_gather(heads, TP, axis=0, tiled=False)]
    reduce_sum x5 -> x0, other arithmetic: 3.57 us -> none  [the longest x2 3.19 us: modulated(): v = v * lax.rsqrt(jnp.mean(v * v, axis=-1, keepdims=True) + EPS)]
  transfers between devices with their start and end apart: 6 -> 2, of which waited for: 6 -> 1; matrix products, arithmetic and copies ran while one was open for 4% -> 5% of each run, Pallas kernels for 0% -> 10%
where the time goes in v2:
time: 150 us
  blocking collectives  69.2 us (46%)
  waiting for transfers between devices  33.2 us (22%)
  Pallas kernels  24.4 us (16%)
  between operations  14.8 us (10%)
  other arithmetic  4.42 us (3%)
  local copies, waits for them, and re-layouts  3.66 us (2%)
    all_gather x1, waiting for transfers between devices, local(): all_heads = lax.all_gather(heads, TP, axis=0, tiled=False)  32.5 us
    all_to_all x1, blocking collectives, local(): lax.all_to_all(partial, SP, split_axis=0, concat_axis=0, tiled=True)  22.9 us
    all_to_all x1, blocking collectives, local(): lax.all_to_all(summed, TP, split_axis=0, concat_axis=0, tiled=True)  18 us
    all_to_all x1, blocking collectives, local(): lax.all_to_all(message, 'z', split_axis=0, concat_axis=0, tiled=True)  17.8 us
    all_to_all x1, blocking collectives, local(): lax.all_to_all(message, 'x', split_axis=0, concat_axis=0, tiled=True)  10.4 us
    pallas_call x1, Pallas kernels, project(): pl.pallas_call(project_body, grid=(cols // tile,), in_specs=[pl.BlockSpec...  9.88 us
    pallas_call x1, Pallas kernels, local(): pl.pallas_call(front_body, grid=(tokens // tile,), in_specs=[pl.BlockSpec...  7.17 us
  transfers between devices with their start and end apart: 2, of which 1 were waited for; matrix products, arithmetic and copies ran while one was open for 5% of the time, Pallas kernels for 10%

profile of v2, /device:TPU:1, one launch (start us, length us, event | category | flops | bytes accessed | tf_op | source)
XLA Modules:
  0.0 149.8 jit_solution(13897490712685982595)
XLA Ops:
  6.5 0.0 copy-start.1
  6.5 0.0 copy-start.2
  6.5 0.0 copy-start.3
  6.5 0.0 copy-start.4
  6.5 0.0 all-gather.4.cloned.1.call-start
  6.6 0.7 all-gather.4.cloned.1.call-update
  7.3 0.0 all-gather.6.cloned.1.call-start
  8.6 1.3 broadcast_in_dim.17.gain_ref
  9.9 0.8 stack.24
  10.7 0.8 stack.25
  11.4 0.1 stack.23
  11.5 0.7 maximum_bitcast_fusion.act_ref
  12.2 1.6 %partial.1 = f32[32,8,128]{2,1,0:T(8,128)} custom-call(bf16[32,2,64]{2,1,0:T(2,128)(2,1)} %maximum_bitcast_fusion.act_ref, s32[1]{0:T(128)} %bitcast.1.at_ref, bf16[64,128]{1,0:T(8,128)(2,1)} %shift_ref.1, bf16[64,128]{1,0:T(8,128)(2,1)} %scale_ref.1, bf16[64,128]{1,0:T(8,128)(2,1)} %gate_ref.1), custom_call_target="tpu_custom_call" | custom-call | tf_op jit(solution)/shard_map/partial/pallas_call | solution.py:277
  13.8 0.1 broadcast_multiply_fusion.1
  13.9 0.1 pad_maximum_fusion.5
  14.0 0.2 broadcast_multiply_fusion
  14.2 0.1 pad_maximum_fusion.3
  14.3 0.9 pad_maximum_fusion.1
  15.2 0.9 pad_maximum_fusion.2
  16.1 0.0 copy-done.1
  16.1 0.0 copy-done.2
  16.1 0.0 copy-done.3
  16.1 0.0 copy-done.4
  16.1 0.0 copy-start
  16.1 1.5 %pad_maximum_fusion.weight_ref = bf16[2048,512]{1,0:T(8,128)(2,1)} fusion(bf16[2048,128]{1,0:T(8,128)(2,1)S(1)} %copy-done.1, bf16[2048,128]{1,0:T(8,128)(2,1)S(1)} %copy-done.2, bf16[2048,128]{1,0:T(8,128)(2,1)S(1)} %copy-done.3, bf16[2048,128]{1,0:T(8,128)(2,1)S(1)} %copy-done.4), kind=kLoop, calls=%fused_computation | loop fusion | flops 8388608 | bytes 4194304 | tf_op jit(solution)/shard_map/concatenate | solution.py:288
  17.7 0.7 broadcast_in_dim.16.par_ref.refs_2_
  18.3 0.0 copy-done
  18.3 22.9 %all_to_all.20.in_ref = f32[32,8,128]{2,1,0:T(8,128)} all-to-all(f32[32,8,128]{2,1,0:T(8,128)S(1)} %copy-done), channel_id=1, replica_groups=mesh['z'=8,'x'=4,'y'=8,'c'=2] {'z','x'}, dimensions={0} | all-to-all | bytes 262144 | tf_op jit(solution)/shard_map/all_to_all | solution.py:299
  41.3 1.6 %sum.1 = f32[16,8,128]{2,1,0:T(8,128)} custom-call(f32[32,8,128]{2,1,0:T(8,128)} %all_to_all.20.in_ref), custom_call_target="tpu_custom_call" | custom-call | tf_op jit(solution)/shard_map/sum/pallas_call | solution.py:300
  42.8 18.0 %all_to_all.21.mod_ref = f32[16,8,128]{2,1,0:T(8,128)} all-to-all(f32[16,8,128]{2,1,0:T(8,128)} %sum.1), channel_id=1, replica_groups=mesh['z'=8,'x'=4,'y'=8,'c'=2] {'y','c'}, dimensions={0} | all-to-all | bytes 131072 | tf_op jit(solution)/shard_map/all_to_all | solution.py:301
  60.9 7.2 %front.1 = (bf16[8,160,128]{2,1,0:T(8,128)(2,1)}, f32[512,128]{1,0:T(8,128)}, bf16[512,128]{1,0:T(8,128)(2,1)}, f32[512,128]{1,0:T(8,128)}, f32[2,128,128]{2,1,0:T(8,128)}, /*index=5*/f32[1,2048]{1,0:T(1,128)}) custom-call(bf16[512,2048]{1,0:T(8,128)(2,1)} %latent_ref.3, bf16[16,2048]{1,0:T(8,128)(2,1)} %context_ref.1, f32[16,8,128]{2,1,0:T(8,128)} %all_to_all.21.mod_ref, ...), custom_call_target="tpu_custom_call" | custom-call | tf_op jit(solution)/shard_map/front/pallas_call | solution.py:306
  68.0 17.8 %all_to_all.22.refs_0_ = bf16[8,160,128]{2,1,0:T(8,128)(2,1)} all-to-all(bf16[8,160,128]{2,1,0:T(8,128)(2,1)} %get-tuple-element.25), channel_id=1, replica_groups=mesh['z'=8,'x'=4,'y'=8,'c'=2] {'z'}, dimensions={0} | all-to-all | bytes 655360 | tf_op jit(solution)/shard_map/all_to_all | solution.py:341
  85.9 2.1 %middle.1 = bf16[4,256,128]{2,1,0:T(8,128)(2,1)} custom-call(bf16[8,160,128]{2,1,0:T(8,128)(2,1)} %all_to_all.22.refs_0_, f32[2,128,128]{2,1,0:T(8,128)} %get-tuple-element.26.refs_1_, f32[8,128]{1,0:T(8,128)} %broadcast_in_dim.16.par_ref.refs_2_), custom_call_target="tpu_custom_call" | custom-call | tf_op jit(solution)/shard_map/middle/pallas_call | solution.py:342
  88.0 10.4 %all_to_all.23.from_ref = bf16[4,256,128]{2,1,0:T(8,128)(2,1)} all-to-all(bf16[4,256,128]{2,1,0:T(8,128)(2,1)} %middle.1), channel_id=1, replica_groups=mesh['z'=8,'x'=4,'y'=8,'c'=2] {'x'}, dimensions={0} | all-to-all | bytes 524288 | tf_op jit(solution)/shard_map/all_to_all | solution.py:347
  98.4 2.2 %finish.1 = bf16[512,128]{1,0:T(8,128)(2,1)} custom-call(bf16[4,256,128]{2,1,0:T(8,128)(2,1)} %all_to_all.23.from_ref, f32[512,128]{1,0:T(8,128)} %get-tuple-element.27.q_ref, bf16[512,128]{1,0:T(8,128)(2,1)} %get-tuple-element.28.g_ref, f32[512,128]{1,0:T(8,128)} %get-tuple-element.29.local_ref, f32[8,128]{1,0:T(8,128)} %broadcast_in_dim.16.par_ref.refs_2_), custom_call_target="tpu_custom_call" | custom-call | tf_op jit(solution)/shard_map/finish/pallas_call | solution.py:348
  100.5 0.0 all-gather.4.cloned.1.call-done.w_ref
  100.5 0.0 all-gather.6.cloned.1.call-update
  100.6 32.5 %all-gather.6.cloned.1.call-done = bf16[8192,128]{1,0:T(8,128)(2,1)} async-done(((bf16[512,128]{1,0:T(8,128)(2,1)}), bf16[8192,128]{1,0:T(8,128)(2,1)}) %all-gather.6.cloned.1.call-update) | async-done | bytes 2097168 | tf_op jit(solution)/shard_map/all_gather | solution.py:352
  133.0 9.9 %project.1 = bf16[512,2048]{1,0:T(8,128)(2,1)} custom-call(bf16[16,512,128]{2,1,0:T(8,128)(2,1)} %bitcast.8, bf16[2048,2048]{1,0:T(8,128)(2,1)} %all-gather.4.cloned.1.call-done.w_ref, bf16[512,2048]{1,0:T(8,128)(2,1)} %latent_ref.3, f32[1,2048]{1,0:T(1,128)} %get-tuple-element.32.gate_ref), custom_call_target="tpu_custom_call" | custom-call | tf_op jit(solution)/shard_map/project/pallas_call | solution.py:228
  (8 shorter events, 0.1 us)
Async XLA Ops:
  6.5 9.6 %copy-start.1 = (bf16[2048,128]{1,0:T(8,128)(2,1)S(1)}, bf16[2048,128]{1,0:T(8,128)(2,1)}, u32[]{:S(2)}) copy-start(bf16[2048,128]{1,0:T(8,128)(2,1)} %param.26) | copy-start | bytes 1572868
  6.5 9.6 %copy-start.2 = (bf16[2048,128]{1,0:T(8,128)(2,1)S(1)}, bf16[2048,128]{1,0:T(8,128)(2,1)}, u32[]{:S(2)}) copy-start(bf16[2048,128]{1,0:T(8,128)(2,1)} %param.25) | copy-start | bytes 1572868
  6.5 9.6 %copy-start.3 = (bf16[2048,128]{1,0:T(8,128)(2,1)S(1)}, bf16[2048,128]{1,0:T(8,128)(2,1)}, u32[]{:S(2)}) copy-start(bf16[2048,128]{1,0:T(8,128)(2,1)} %param.24) | copy-start | bytes 1572868
  6.5 9.6 %copy-start.4 = (bf16[2048,128]{1,0:T(8,128)(2,1)S(1)}, bf16[2048,128]{1,0:T(8,128)(2,1)}, u32[]{:S(2)}) copy-start(bf16[2048,128]{1,0:T(8,128)(2,1)} %param.23) | copy-start | bytes 1572868
  6.5 94.0 %all-gather.4.cloned.1.call-start = ((), (), s32[]{:S(2)}) async-start(), calls=%async_computation.4 | async-start | bytes 8912896 | tf_op jit(solution)/shard_map/all_gather | solution.py:272
  7.3 125.8 %all-gather.6.cloned.1.call-start = ((), (), s32[]{:S(2)}) async-start(), calls=%async_computation.5 | async-start | bytes 2228224 | tf_op jit(solution)/shard_map/all_gather | solution.py:352
  16.1 2.2 %copy-start = (f32[32,8,128]{2,1,0:T(8,128)S(1)}, f32[32,8,128]{2,1,0:T(8,128)}, u32[]{:S(2)}) copy-start(f32[32,8,128]{2,1,0:T(8,128)} %partial.1) | copy-start | bytes 393220
Sparse Core Ops, SparseCore 0:
  9.5 65.4 all-gather.3
  100.7 32.3 all-gather.5
